TPU v7x, 32 devices: a whole 2x2x4 slice. The times are simulated.
32 devices in a mesh: sp: 8 (over z, x), tp: 4 (over y, core).
Axes of the slice: x: 2, y: 2, z: 4, core: 2. Of those that a mesh axis runs over, the one named last changes fastest.
Arguments:
- incoming_residual_stream: bfloat16 [4096, 2048], P(('sp', 'tp')), may hold values from -6 to 6
- result_valve: bfloat16 [4096, 2048], P('sp', 'tp'), may hold values from -6 to 6
- channel_feed_matrix: bfloat16 [4096, 2048], P('sp', 'tp'), may hold values from -6 to 6
- memory_feed_matrix: bfloat16 [4096, 512], P('sp', 'tp'), may hold values from -6 to 6
- memory_query_matrix: bfloat16 [4096, 512], P('sp', 'tp'), may hold values from -6 to 6
- unsoftened_deltas: float32 [4096, 32], P('sp', 'tp'), may hold values from -2.7 to 2.7
- delta_offset: float32 [32], P('tp'), may hold values from -4.5 to -3.5
- channel_fading_speed: float32 [32], P('tp'), as said below
- extra_log_fading: float32 [4096, 32], P('sp', 'tp'), may hold values from -0.7 to 0
- bypass_factor: float32 [32], P('tp'), may hold values from 0.1 to 1.9
- channel_feed_kernel: bfloat16 [4, 2048], P(None, 'tp'), may hold values from -3 to 3
- memory_feed_kernel: bfloat16 [4, 512], P(None, 'tp'), may hold values from -3 to 3
- memory_query_kernel: bfloat16 [4, 512], P(None, 'tp'), may hold values from -3 to 3
- cluster_scaling_vector: float32 [2048], P('tp'), may hold values from 0.1 to 1.9
- mixer_result_matrix: bfloat16 [2048, 2048], P('tp'), may hold values from -0.125 to 0.125
- initial_scaling_vector: float32 [2048], replicated, may hold values from 0.1 to 1.9
- valve_matrix: bfloat16 [2048, 5632], P('sp', 'tp'), may hold values from -0.125 to 0.125
- widen_matrix: bfloat16 [2048, 5632], P('sp', 'tp'), may hold values from -0.125 to 0.125
- shrink_matrix: bfloat16 [5632, 2048], P('tp', 'sp'), may hold values from -0.078125 to 0.078125
- valve_filter_kernel: bfloat16 [3, 5632], P(None, 'tp'), may hold values from -3.5 to 3.5
- widen_filter_kernel: bfloat16 [3, 5632], P(None, 'tp'), may hold values from -3.5 to 3.5
- latter_scaling_vector: float32 [2048], replicated, may hold values from 0.1 to 1.9
Outputs:
- layer_out: bfloat16 [4096, 2048], P(('sp', 'tp'))
Inputs may be any that keep to these rules, and one draw needn't show every extreme that they name: `channel_fading_speed`: positive.
All inputs are finite; a program needn't handle non-finite values.
Results may differ from a plain program's by a relative error of at most 0.02.
Values may be sent and summed in bfloat16 or wider, within the bound.
A program may use at most 128 MiB of HBM per device.

v0:
```python
import jax
import jax.numpy as jnp
from jax import lax
from jax.sharding import PartitionSpec as P

HEADS = 32
HEAD_DIM = 64
GROUPS = 4
STATE = 128
CONV = 4
FCONV = 3
BLOCK = 128


EPSILON = 1e-05
ALPHA = 2.0**0.25
HIGHEST = lax.Precision.HIGHEST


def shifted(shard, axis, by):
    count = lax.axis_size(axis)
    pairs = [(i, i + by) for i in range(count) if 0 <= i + by < count]
    return lax.ppermute(shard, axis, pairs)


def entering(shard, axis, join, neutral):
    place = lax.axis_index(axis)
    gathered = jax.tree.map(
        lambda a, kind: lax.all_gather(a.astype(kind), axis), shard, (jnp.bfloat16, jnp.bfloat16)
    )
    state = jax.tree.map(lambda a, e: jnp.zeros_like(a) + jnp.asarray(e, a.dtype), shard, neutral)

    def one(lap, state):
        return join(
            state,
            jax.tree.map(
                lambda a, own: lax.dynamic_index_in_dim(a, lap, 0, False).astype(own.dtype),
                gathered,
                shard,
            ),
        )

    return lax.fori_loop(0, place, one, state)


def causal_conv(signal, before, tap_weights):
    tap_count = tap_weights.shape[0]
    row_count = signal.shape[0]
    padded = jnp.concatenate([before, signal], axis=0).astype(jnp.float32)
    running = jnp.zeros(signal.shape, jnp.float32)
    for tap_index in range(tap_count):
        running = (
            running
            + tap_weights[tap_index].astype(jnp.float32) * padded[tap_index : tap_index + row_count]
        )
    return running


def layer_norm(values, scales):
    row_mean = jnp.mean(values, axis=-1, keepdims=True)
    centred = values - row_mean
    spread = jnp.mean(centred * centred, axis=-1, keepdims=True)
    return centred * lax.rsqrt(spread + EPSILON) * scales


def combine_states(earlier_pair, later_pair):
    return (
        earlier_pair[0] * later_pair[1][..., None, None] + later_pair[0],
        earlier_pair[1] * later_pair[1],
    )


def chain_step(state_now, inputs):
    fresh_one, decay_one = inputs
    return (state_now * decay_one[..., None, None] + fresh_one, state_now)


def shards(
    incoming_residual_stream,
    result_valve,
    channel_feed_matrix,
    memory_feed_matrix,
    memory_query_matrix,
    unsoftened_deltas,
    delta_offset,
    channel_fading_speed,
    extra_log_fading,
    bypass_factor,
    channel_feed_kernel,
    memory_feed_kernel,
    memory_query_kernel,
    cluster_scaling_vector,
    mixer_result_matrix,
    initial_scaling_vector,
    valve_matrix,
    widen_matrix,
    shrink_matrix,
    valve_filter_kernel,
    widen_filter_kernel,
    latter_scaling_vector,
):
    row_count = channel_feed_matrix.shape[0]
    inner_here = channel_feed_matrix.shape[1]
    group_count = memory_feed_matrix.shape[1] // STATE
    group_heads = HEADS // GROUPS
    block_count = row_count // BLOCK
    rim_rows = CONV - 1
    rim_x, rim_b, rim_c = shifted(
        (
            channel_feed_matrix[row_count - rim_rows :],
            memory_feed_matrix[row_count - rim_rows :],
            memory_query_matrix[row_count - rim_rows :],
        ),
        "sp",
        1,
    )
    x_act = jax.nn.silu(causal_conv(channel_feed_matrix, rim_x, channel_feed_kernel)).astype(
        jnp.bfloat16
    )
    b_act = jax.nn.silu(causal_conv(memory_feed_matrix, rim_b, memory_feed_kernel)).astype(
        jnp.bfloat16
    )
    c_act = jax.nn.silu(causal_conv(memory_query_matrix, rim_c, memory_query_kernel)).astype(
        jnp.bfloat16
    )
    channel_delta_amount = jax.nn.softplus(unsoftened_deltas + delta_offset[None, :])
    log_fading_amount = extra_log_fading - channel_fading_speed[None, :] * channel_delta_amount
    x_heads = x_act.astype(jnp.float32).reshape(row_count, group_count, group_heads, HEAD_DIM)
    x_scaled = (
        x_heads * channel_delta_amount.reshape(row_count, group_count, group_heads)[..., None]
    )
    b_full = b_act.astype(jnp.float32).reshape(row_count, group_count, STATE)
    c_full = c_act.astype(jnp.float32).reshape(row_count, group_count, STATE)
    decay_full = log_fading_amount.reshape(row_count, group_count, group_heads)
    x_blk = x_scaled.reshape(block_count, BLOCK, group_count, group_heads, HEAD_DIM)
    b_blk = b_full.reshape(block_count, BLOCK, group_count, STATE)
    c_blk = c_full.reshape(block_count, BLOCK, group_count, STATE)
    b_narrow = b_act.reshape(block_count, BLOCK, group_count, STATE)
    c_narrow = c_act.reshape(block_count, BLOCK, group_count, STATE)
    decay_blk = decay_full.reshape(block_count, BLOCK, group_count, group_heads)
    cum_decay = jnp.cumsum(decay_blk, axis=1)
    causal = jnp.tril(jnp.ones((BLOCK, BLOCK), dtype=bool))
    between = cum_decay[:, :, None] - cum_decay[:, None, :]
    lag = jnp.exp(jnp.where(causal[None, :, :, None, None], between, -jnp.inf))
    affinity = jnp.einsum("blgn,bsgn->blsg", c_narrow, b_narrow, preferred_element_type=jnp.float32)
    mixing = affinity[..., None] * lag
    within = jnp.einsum("blsgh,bsghp->blghp", mixing, x_blk, precision=HIGHEST)
    to_end = jnp.exp(cum_decay[:, -1:] - cum_decay)
    fresh = jnp.einsum("blgn,blghp->bghpn", b_blk, x_blk * to_end[..., None], precision=HIGHEST)
    block_decay = jnp.exp(cum_decay[:, -1])
    initial = jnp.zeros((group_count, group_heads, HEAD_DIM, STATE), jnp.float32)
    local_end, earlier = lax.scan(chain_step, initial, (fresh, block_decay))
    carried = (
        jnp.einsum("blgn,bghpn->blghp", c_blk, earlier, precision=HIGHEST)
        * jnp.exp(cum_decay)[..., None]
    )
    from_start = jnp.cumsum(decay_full, axis=0)
    incoming, _ = entering(
        (local_end, jnp.exp(from_start[-1])),
        "sp",
        combine_states,
        (jnp.zeros_like(local_end), jnp.ones_like(from_start[-1])),
    )
    arriving = (
        jnp.einsum("tgn,ghpn->tghp", c_full, incoming, precision=HIGHEST)
        * jnp.exp(from_start)[..., None]
    )
    y_heads = (within + carried).reshape(row_count, group_count, group_heads, HEAD_DIM) + arriving
    y_heads = y_heads + bypass_factor.reshape(group_count, group_heads)[None, :, :, None] * x_heads
    gated = y_heads.reshape(row_count, group_count, group_heads * HEAD_DIM)
    gated = gated * jax.nn.silu(result_valve.astype(jnp.float32)).reshape(
        row_count, group_count, group_heads * HEAD_DIM
    )
    gated = gated * lax.rsqrt(jnp.mean(gated * gated, axis=-1, keepdims=True) + EPSILON)
    y_norm = (gated.reshape(row_count, inner_here) * cluster_scaling_vector[None, :]).astype(
        jnp.bfloat16
    )
    mixer = lax.psum_scatter(
        jnp.dot(y_norm, mixer_result_matrix, preferred_element_type=jnp.float32).astype(
            jnp.bfloat16
        ),
        "tp",
        scatter_dimension=0,
        tiled=True,
    ).astype(jnp.float32)
    normed_own = layer_norm(
        ALPHA * incoming_residual_stream.astype(jnp.float32) + mixer, initial_scaling_vector
    ).astype(jnp.bfloat16)
    normed_all = lax.all_gather(normed_own, "tp", axis=0, tiled=True)
    gate_sum = jnp.dot(
        normed_all,
        lax.all_gather(valve_matrix, "sp", axis=0, tiled=True),
        preferred_element_type=jnp.float32,
    )
    up_sum = jnp.dot(
        normed_all,
        lax.all_gather(widen_matrix, "sp", axis=0, tiled=True),
        preferred_element_type=jnp.float32,
    )
    gate_proj = gate_sum.astype(jnp.bfloat16)
    up_proj = up_sum.astype(jnp.bfloat16)
    ffn_rows = FCONV - 1
    rim_gate, rim_up = shifted(
        (gate_proj[row_count - ffn_rows :], up_proj[row_count - ffn_rows :]), "sp", 1
    )
    gate_conv = causal_conv(gate_proj, rim_gate, valve_filter_kernel)
    up_conv = causal_conv(up_proj, rim_up, widen_filter_kernel)
    hidden = (jax.nn.silu(gate_conv) * up_conv).astype(jnp.bfloat16)
    channel_part = jnp.dot(
        hidden,
        lax.all_gather(shrink_matrix, "sp", axis=1, tiled=True),
        preferred_element_type=jnp.float32,
    )
    channel = lax.psum_scatter(
        channel_part.astype(jnp.bfloat16), "tp", scatter_dimension=0, tiled=True
    ).astype(jnp.float32)
    return layer_norm(
        ALPHA * normed_own.astype(jnp.float32) + channel, latter_scaling_vector
    ).astype(jnp.bfloat16)


def solution(mesh):
    in_specs = (
        P(("sp", "tp"), None),
        P("sp", "tp"),
        P("sp", "tp"),
        P("sp", "tp"),
        P("sp", "tp"),
        P("sp", "tp"),
        P("tp"),
        P("tp"),
        P("sp", "tp"),
        P("tp"),
        P(None, "tp"),
        P(None, "tp"),
        P(None, "tp"),
        P("tp"),
        P("tp", None),
        P(),
        P("sp", "tp"),
        P("sp", "tp"),
        P("tp", "sp"),
        P(None, "tp"),
        P(None, "tp"),
        P(),
    )
    out_specs = P(("sp", "tp"), None)
    return jax.shard_map(shards, mesh=mesh, in_specs=in_specs, out_specs=out_specs, check_vma=False)
```

profile of v0, /device:TPU:25, one launch (start us, length us, event | category | flops | bytes accessed | tf_op | source)
XLA Modules:
  0.0 505.8 jit_solution(13822503605114422676)
XLA Ops:
  7.9 3.1 collective-permute-start.2
  32.8 2.5 broadcast_multiply_fusion
  36.8 9.7 %while.26 = (s32[]{:T(128)}, f32[1,8,64,128]{3,2,1,0:T(8,128)S(1)}, f32[4,1,8,64,128]{4,3,2,1,0:T(8,128)}, f32[4,1,8]{2,1,0:T(1,128)}, f32[4,1,8,64,128]{4,3,2,1,0:T(8,128)}, /*index=5*/s32[]{:T(128)}, s32[]{:T(128)}) while((s32[]{:T(128)}, f32[1,8,64,128]{3,2,1,0:T(8,128)S(1)}, f32[4,1,8,64,128]{4,3,2,1,0:T(8,128)}, ...), condition=%wide.region_2.3_spmd.clone, body=%wide.region_1.2_spmd.clone.sunk | while | flops 262147 | bytes 1311424 | solution.py:152
  53.0 13.3 %all_gather.22 = bf16[8,1,8]{2,1,0:T(2,128)(2,1)} all-gather(bf16[1,1,8]{2,1,0:T(2,128)(2,1)S(1)} %copy.70), channel_id=1, replica_groups=mesh['sp'=8,'tp'=4] {'sp'}, dimensions={0}, use_global_device_ids=true | all-gather | bytes 144 | tf_op jit(solution)/shard_map/all_gather | solution.py:29
  69.2 5.5 %fusion.13 = f32[4,128,1,8,64]{1,4,3,0,2:T(8,128)S(1)} fusion(f32[4,128,8,64]{1,0,3,2:T(4,128)} %get-tuple-element.157, f32[4,128,8]{1,2,0:T(8,128)} %copy.60, f32[4,128,128]{2,1,0:T(8,128)} %copy.58, pred[128,128]{1,0:T(8,128)(4,1)} %iota_compare_fusion), kind=kOutput, calls=%fused_computation.30 | convolution fusion | flops 404226048 | bytes 2392064 | tf_op jit(solution)/shard_map/blsgh,bsghp->blghp/dot_general | solution.py:147
  77.1 9.6 %all-gather.15.cloned.1.call-done = bf16[8,8,64,128]{3,2,1,0:T(8,128)(2,1)} async-done(((bf16[1,8,64,128]{3,2,1,0:T(8,128)(2,1)}), bf16[8,8,64,128]{3,2,1,0:T(8,128)(2,1)}) %all-gather.15.cloned.1.call-update) | async-done | bytes 1048592 | tf_op jit(solution)/shard_map/all_gather | solution.py:29
  86.7 10.0 %while.25 = (s32[]{:T(128)}, f32[1,8,64,128]{3,2,1,0:T(8,128)S(1)}, s32[]{:T(128)}, bf16[8,1,8]{2,1,0:T(2,128)(2,1)}, bf16[8,1,8,64,128]{4,3,2,1,0:T(8,128)(2,1)}, /*index=5*/s32[]{:T(128)}, s32[]{:T(128)}, s32[]{:T(128)}) while((s32[]{:T(128)}, f32[1,8,64,128]{3,2,1,0:T(8,128)S(1)}, s32[]{:T(128)}, bf16[8,1,8]{2,1,0:T(2,128)(2,1)}, ...), condition=%wide.region_6.7_spmd, body=%wide.region_5.6_spmd.sunk | while | flops 196621 | bytes 655567 | solution.py:43
  96.8 2.9 fusion.18
  103.1 4.2 convolution_convert_fusion.2
  107.6 34.7 %reduce-scatter.3.cloned.1.call-done = bf16[128,2048]{1,0:T(8,128)(2,1)} async-done(((bf16[512,2048]{1,0:T(8,128)(2,1)}), bf16[128,2048]{1,0:T(8,128)(2,1)}) %reduce-scatter.3.cloned.1.call-update) | async-done | bytes 524304 | tf_op jit(solution)/shard_map/reduce_scatter | solution.py:178
  145.0 2.1 multiply_convert_fusion.1
  149.6 20.8 %all-gather.7.cloned.1.call-done = bf16[512,2048]{1,0:T(8,128)(2,1)} async-done(((bf16[128,2048]{1,0:T(8,128)(2,1)}), bf16[512,2048]{1,0:T(8,128)(2,1)}) %all-gather.7.cloned.1.call-update) | async-done | bytes 2097168 | tf_op jit(solution)/shard_map/all_gather | solution.py:189
  170.4 92.2 %all-gather.9.cloned.1.call-done = bf16[2048,1408]{1,0:T(8,128)(2,1)} async-done(((bf16[256,1408]{1,0:T(8,128)(2,1)}), bf16[2048,1408]{1,0:T(8,128)(2,1)}) %all-gather.9.cloned.1.call-update) | async-done | bytes 5767184 | tf_op jit(solution)/shard_map/all_gather | solution.py:192
  262.5 6.7 %convolution_convert_fusion.1 = bf16[512,1408]{1,0:T(8,128)(2,1)S(1)} fusion(bf16[512,2048]{1,0:T(8,128)(2,1)} %all-gather.7.cloned.1.call-done, bf16[2048,1408]{1,0:T(8,128)(2,1)} %all-gather.9.cloned.1.call-done), kind=kOutput, calls=%fused_computation.7 | convolution fusion | flops 2953510912 | bytes 9306112 | tf_op jit(solution)/shard_map/dot_general | solution.py:190
  269.8 2.2 collective-permute-start.3
  272.0 83.1 %all-gather.11.cloned.1.call-done = bf16[2048,1408]{1,0:T(8,128)(2,1)} async-done(((bf16[256,1408]{1,0:T(8,128)(2,1)}), bf16[2048,1408]{1,0:T(8,128)(2,1)}) %all-gather.11.cloned.1.call-update) | async-done | bytes 5767184 | tf_op jit(solution)/shard_map/all_gather | solution.py:197
  355.1 6.7 %convolution_convert_fusion = bf16[512,1408]{1,0:T(8,128)(2,1)S(1)} fusion(bf16[512,2048]{1,0:T(8,128)(2,1)} %all-gather.7.cloned.1.call-done, bf16[2048,1408]{1,0:T(8,128)(2,1)} %all-gather.11.cloned.1.call-done), kind=kOutput, calls=%fused_computation.6 | convolution fusion | flops 2953510912 | bytes 9306112 | tf_op jit(solution)/shard_map/dot_general | solution.py:195
  361.9 2.2 collective-permute-start.4
  364.0 2.6 maximum_convert_fusion
  367.1 1.9 maximum_convert_fusion.1
  369.1 79.4 %all-gather.13.cloned.1.call-done = bf16[1408,2048]{1,0:T(8,128)(2,1)} async-done(((bf16[1408,256]{1,0:T(8,128)(2,1)}), bf16[1408,2048]{1,0:T(8,128)(2,1)}) %all-gather.13.cloned.1.call-update) | async-done | bytes 5767184 | tf_op jit(solution)/shard_map/all_gather | solution.py:211
  448.5 14.5 %convolution_convert_fusion.3 = bf16[512,2048]{1,0:T(8,128)(2,1)} fusion(bf16[1408,2048]{1,0:T(8,128)(2,1)} %all-gather.13.cloned.1.call-done, f32[514,1408]{1,0:T(8,128)} %maximum_convert_fusion.1, f32[514,1408]{1,0:T(8,128)} %maximum_convert_fusion, f32[1408]{0:T(1024)S(1)} %get-tuple-element.132, f32[1408]{0:T(1024)S(1)} %copy-done.18, ...), kind=kOutput, calls=%fused_computation.9 | convolution fusion | flops 2965372928 | bytes 25199616 | tf_op jit(solution)/shard_map/dot_general | solution.py:209
  463.0 31.2 %reduce-scatter.5.cloned.1.call-done = bf16[128,2048]{1,0:T(8,128)(2,1)} async-done(((bf16[512,2048]{1,0:T(8,128)(2,1)}), bf16[128,2048]{1,0:T(8,128)(2,1)}) %reduce-scatter.5.cloned.1.call-update) | async-done | bytes 524304 | tf_op jit(solution)/shard_map/reduce_scatter | solution.py:214
  496.9 2.1 multiply_convert_fusion
  (145 shorter events, 68.2 us)
Async XLA Ops:
  6.5 96.5 %copy-start = (bf16[512,2048]{1,0:T(8,128)(2,1)S(1)}, bf16[512,2048]{1,0:T(8,128)(2,1)}, u32[]{:S(2)}) copy-start(bf16[512,2048]{1,0:T(8,128)(2,1)} %param.40) | copy-start | bytes 6291460
  6.5 20.9 %copy-start.7 = (bf16[512,512]{1,0:T(8,128)(2,1)S(1)}, bf16[512,512]{1,0:T(8,128)(2,1)}, u32[]{:S(2)}) copy-start(bf16[512,512]{1,0:T(8,128)(2,1)} %param.28) | copy-start | bytes 1572868
  6.5 80.1 %all-gather.15.cloned.1.call-start = ((), (), s32[]{:S(2)}) async-start(), calls=%async_computation.8 | async-start | bytes 1179648 | tf_op jit(solution)/shard_map/all_gather | solution.py:29
  7.9 58.4 %collective-permute-start.2 = (bf16[3,128]{1,0:T(4,128)(2,1)}, bf16[3,128]{1,0:T(4,128)(2,1)}, u32[]{:S(2)}, u32[]{:S(2)}) collective-permute-start(bf16[3,128]{1,0:T(4,128)(2,1)} %slice.155), channel_id=1, source_target_pairs={{0,4},{4,8},{8,12},{12,16},{16,20},{20,24},{24,28},{1,5},{5,9},{9,... | collective-permute-start | bytes 2312 | tf_op jit(solution)/shard_map/ppermute | solution.py:23
  11.7 13.9 %collective-permute-start.1 = (bf16[3,128]{1,0:T(4,128)(2,1)S(1)}, bf16[3,128]{1,0:T(4,128)(2,1)S(1)}, u32[]{:S(2)}, u32[]{:S(2)}) collective-permute-start(bf16[3,128]{1,0:T(4,128)(2,1)S(1)} %slice.146), channel_id=1, source_target_pairs={{0,4},{4,8},{8,12},{12,16},{16,20},{20,24},{24,28},{1,5},{5,9},{9,... | collective-permute-start | bytes 2312 | tf_op jit(solution)/shard_map/ppermute | solution.py:23
  14.9 12.5 %collective-permute-start = (bf16[3,512]{1,0:T(4,128)(2,1)}, bf16[3,512]{1,0:T(4,128)(2,1)}, u32[]{:S(2)}, u32[]{:S(2)}) collective-permute-start(bf16[3,512]{1,0:T(4,128)(2,1)} %slice.137), channel_id=1, source_target_pairs={{0,4},{4,8},{8,12},{12,16},{16,20},{20,24},{24,28},{1,5},{5,9},{9,... | collective-permute-start | bytes 9224 | tf_op jit(solution)/shard_map/ppermute | solution.py:23
  36.8 29.5 %copy-start.8 = (bf16[512,128]{1,0:T(8,128)(2,1)S(1)}, bf16[512,128]{1,0:T(8,128)(2,1)}, u32[]{:S(2)}) copy-start(bf16[512,128]{1,0:T(8,128)(2,1)} %param.30) | copy-start | bytes 393220
  47.2 95.0 %reduce-scatter.3.cloned.1.call-start = ((), (), s32[]{:S(2)}) async-start(), calls=%async_computation.2 | async-start | bytes 2621440 | tf_op jit(solution)/shard_map/reduce_scatter | solution.py:178
  75.4 21.3 %copy-start.9 = (f32[512,8]{0,1:T(8,128)S(1)}, f32[512,8]{0,1:T(8,128)}, u32[]{:S(2)}) copy-start(f32[512,8]{0,1:T(8,128)} %get-tuple-element.154) | copy-start | bytes 49156
  103.1 39.2 %copy-start.2 = (bf16[128,2048]{1,0:T(8,128)(2,1)S(1)}, bf16[128,2048]{1,0:T(8,128)(2,1)}, u32[]{:S(2)}) copy-start(bf16[128,2048]{1,0:T(8,128)(2,1)} %param.26) | copy-start | bytes 1572868
  107.3 37.6 %copy-start.16 = (f32[2048]{0:T(1024)S(1)}, f32[2048]{0:T(1024)}, u32[]{:S(2)}) copy-start(f32[2048]{0:T(1024)} %param.41) | copy-start | bytes 24580
  107.3 63.0 %all-gather.7.cloned.1.call-start = ((), (), s32[]{:S(2)}) async-start(), calls=%async_computation.3 | async-start | bytes 2621440 | tf_op jit(solution)/shard_map/all_gather | solution.py:189
  147.1 115.4 %all-gather.9.cloned.1.call-start = ((), (), s32[]{:S(2)}) async-start(), calls=%async_computation.4 | async-start | bytes 6488064 | tf_op jit(solution)/shard_map/all_gather | solution.py:192
  147.7 207.5 %all-gather.11.cloned.1.call-start = ((), (), s32[]{:S(2)}) async-start(), calls=%async_computation.5 | async-start | bytes 6488064 | tf_op jit(solution)/shard_map/all_gather | solution.py:197
  148.3 300.2 %all-gather.13.cloned.1.call-start = ((), (), s32[]{:S(2)}) async-start(), calls=%async_computation.6 | async-start | bytes 6488064 | tf_op jit(solution)/shard_map/all_gather | solution.py:211
  148.9 345.3 %reduce-scatter.5.cloned.1.call-start = ((), (), s32[]{:S(2)}) async-start(), calls=%async_computation.7 | async-start | bytes 2621440 | tf_op jit(solution)/shard_map/reduce_scatter | solution.py:214
  269.8 94.2 %collective-permute-start.3 = (bf16[2,1408]{1,0:T(2,128)(2,1)}, bf16[2,1408]{1,0:T(2,128)(2,1)}, u32[]{:S(2)}, u32[]{:S(2)}) collective-permute-start(bf16[2,1408]{1,0:T(2,128)(2,1)} %slice.196), channel_id=1, source_target_pairs={{0,4},{4,8},{8,12},{12,16},{16,20},{20,24},{24,28},{1,5},{5,9},{9,... | collective-permute-start | bytes 16904 | tf_op jit(solution)/shard_map/ppermute | solution.py:23
  361.9 5.3 %collective-permute-start.4 = (bf16[2,1408]{1,0:T(2,128)(2,1)S(1)}, bf16[2,1408]{1,0:T(2,128)(2,1)S(1)}, u32[]{:S(2)}, u32[]{:S(2)}) collective-permute-start(bf16[2,1408]{1,0:T(2,128)(2,1)S(1)} %slice.200), channel_id=1, source_target_pairs={{0,4},{4,8},{8,12},{12,16},{16,20},{20,24},{24,28},{1,5},{5,9},{9,... | collective-permute-start | bytes 16904 | tf_op jit(solution)/shard_map/ppermute | solution.py:23
  366.7 81.8 %copy-start.18 = (f32[1408]{0:T(1024)S(1)}, f32[1408]{0:T(1024)}, u32[]{:S(2)}) copy-start(f32[1408]{0:T(1024)} %get-tuple-element.133) | copy-start | bytes 16900
  366.7 81.8 %copy-start.19 = (f32[1408]{0:T(1024)S(1)}, f32[1408]{0:T(1024)}, u32[]{:S(2)}) copy-start(f32[1408]{0:T(1024)} %get-tuple-element.177) | copy-start | bytes 16900
  366.7 81.8 %copy-start.20 = (f32[1408]{0:T(1024)S(1)}, f32[1408]{0:T(1024)}, u32[]{:S(2)}) copy-start(f32[1408]{0:T(1024)} %get-tuple-element.178) | copy-start | bytes 16900
  366.7 81.8 %copy-start.21 = (f32[1408]{0:T(1024)S(1)}, f32[1408]{0:T(1024)}, u32[]{:S(2)}) copy-start(f32[1408]{0:T(1024)} %get-tuple-element.179) | copy-start | bytes 16900
  448.5 45.7 %copy-start.1 = (bf16[128,2048]{1,0:T(8,128)(2,1)S(1)}, bf16[128,2048]{1,0:T(8,128)(2,1)}, u32[]{:S(2)}) copy-start(bf16[128,2048]{1,0:T(8,128)(2,1)} %multiply_convert_fusion.1) | copy-start | bytes 1572868
  463.0 33.9 %copy-start.17 = (f32[2048]{0:T(1024)S(1)}, f32[2048]{0:T(1024)}, u32[]{:S(2)}) copy-start(f32[2048]{0:T(1024)} %param.47) | copy-start | bytes 24580
  (11 other events, 51.6 us)
Sparse Core Ops, SparseCore 0:
  47.4 39.2 all-gather.14
  107.5 34.7 reduce-scatter.2
  147.2 23.1 all-gather.6
  172.4 90.0 all-gather.8
  264.6 90.5 all-gather.10
  357.0 91.3 all-gather.12
  463.1 30.9 reduce-scatter.4
where the time goes:
time: 509 us; the launch traced here: 506 us
  waiting for transfers between devices  353 us (69%)
  other arithmetic  50.6 us (10%)
  matrix products  43.8 us (9%)
  local copies, waits for them, and re-layouts  19.3 us (4%)
  between operations  13.9 us (3%)
  blocking collectives  13.3 us (3%)
  starting transfers between devices  11.7 us (2%)
    all_gather x1, waiting for transfers between devices, shards(): lax.all_gather(valve_matrix, 'sp', axis=0, tiled=True)  92.2 us
    all_gather x1, waiting for transfers between devices, shards(): lax.all_gather(widen_matrix, 'sp', axis=0, tiled=True)  83.1 us
    all_gather x1, waiting for transfers between devices, shards(): lax.all_gather(shrink_matrix, 'sp', axis=1, tiled=True)  79.4 us
    reduce_scatter x1, waiting for transfers between devices, shards(): lax.psum_scatter(jnp.dot(y_norm, mixer_result_matrix, preferred_element_t...  34.7 us
    reduce_scatter x1, waiting for transfers between devices, shards(): lax.psum_scatter(channel_part.astype(jnp.bfloat16), 'tp', scatter_dimensi...  31.2 us
    all_gather x1, waiting for transfers between devices, shards(): normed_all = lax.all_gather(normed_own, 'tp', axis=0, tiled=True)  20.8 us
    dot_general x1, matrix products, shards(): jnp.dot(hidden, lax.all_gather(shrink_matrix, 'sp', axis=1, tiled=True),...  14.5 us
    all_gather x1, blocking collectives, entering(): lax.all_gather(a.astype(kind), axis)  13.3 us
  transfers between devices with their start and end apart: 12, of which 8 were waited for; matrix products, arithmetic and copies ran while one was open for 13% of the time, Pallas kernels for 0%

commit v1 on v0

--- a/solution.py
+++ b/solution.py
@@ -1,6 +1,9 @@
+import functools
 import jax
 import jax.numpy as jnp
 from jax import lax
+from jax.experimental import pallas as pl
+from jax.experimental.pallas import tpu as pltpu
 from jax.sharding import PartitionSpec as P
 
 HEADS = 32
@@ -75,7 +78,7 @@
     return (state_now * decay_one[..., None, None] + fresh_one, state_now)
 
 
-def shards(
+def plain_shards(
     incoming_residual_stream,
     result_valve,
     channel_feed_matrix,
@@ -219,6 +222,553 @@
     ).astype(jnp.bfloat16)
 
 
+MESH = pl.DeviceIdType.MESH
+RIM = 16
+
+
+def silu(v):
+    return v / (1.0 + jnp.exp(-v))
+
+
+def layer_kernel(
+    n_sp,
+    n_tp,
+    res_ref,
+    rv_ref,
+    xf_ref,
+    bf_ref,
+    cf_ref,
+    dt_ref,
+    doff_ref,
+    fade_ref,
+    elf_ref,
+    byp_ref,
+    xk_ref,
+    bk_ref,
+    ck_ref,
+    csv_ref,
+    mm_ref,
+    g1_ref,
+    v_hbm,
+    w_hbm,
+    s_hbm,
+    vk_ref,
+    wk_ref,
+    g2_ref,
+    out_ref,
+    v_all,
+    w_all,
+    s_all,
+    rim_x,
+    rim_b,
+    rim_c,
+    ext,
+    x_act,
+    b_act,
+    c_act,
+    step_ref,
+    ld_ref,
+    y_ref,
+    efs_ref,
+    base_ref,
+    state_ref,
+    st_send,
+    dec_send,
+    st_recv,
+    dec_recv,
+    part,
+    recv1,
+    recv2,
+    normed,
+    hidden,
+    own_sem,
+    ring_send,
+    ring_recv,
+    rim_send,
+    rim_recv,
+    st_ssem,
+    st_rsem,
+    t1_send,
+    t1_recv,
+    t2_send,
+    t2_recv,
+    t3_send,
+    t3_recv,
+    nr_send,
+    nr_recv,
+):
+    f32, bf16 = jnp.float32, jnp.bfloat16
+    rows, inner = xf_ref.shape
+    heads = dt_ref.shape[1]
+    own_rows = rows // n_tp
+    width = mm_ref.shape[1]
+    ff = v_hbm.shape[1]
+    depth = v_hbm.shape[0]
+    cols = s_hbm.shape[1]
+    blocks = rows // BLOCK
+    me = lax.axis_index("sp")
+    mt = lax.axis_index("tp")
+    half = n_sp // 2
+
+    def owner(pos):
+        back = pos // half
+        return (1 - back) * 2 * pos + back * (2 * (n_sp - 1 - pos) + 1)
+
+    odd = me % 2
+    place = (1 - odd) * (me // 2) + odd * (n_sp - 1 - me // 2)
+    after = owner((place + 1) % n_sp)
+    ahead = owner((place + n_sp - 1) % n_sp)
+
+    barrier = pltpu.get_barrier_semaphore()
+    for d in range(1, n_sp):
+        pl.semaphore_signal(barrier, inc=1, device_id=((me + d) % n_sp, mt), device_id_type=MESH)
+    for d in range(1, n_tp):
+        pl.semaphore_signal(barrier, inc=1, device_id=(me, (mt + d) % n_tp), device_id_type=MESH)
+    pl.semaphore_wait(barrier, n_sp + n_tp - 2)
+
+    def slot(piece, who):
+        if piece == 2:
+            return s_all.at[who]
+        whole = v_all if piece == 0 else w_all
+        return whole.at[pl.ds(pl.multiple_of(who * depth, depth), depth)]
+
+    sources = (v_hbm, w_hbm, s_hbm)
+    hops = {}
+    for piece in range(3):
+        long_way = half if piece != 1 else n_sp - 1 - half
+        hops[piece] = (long_way, n_sp - 1 - long_way)
+
+    def ring_copy(piece, way, step):
+        who = owner((place + n_sp - step) % n_sp if way == 0 else (place + step) % n_sp)
+        return pltpu.make_async_remote_copy(
+            src_ref=sources[piece] if step == 0 else slot(piece, who),
+            dst_ref=slot(piece, who),
+            send_sem=ring_send.at[way, step, piece],
+            recv_sem=ring_recv.at[way, step, piece],
+            device_id=(after if way == 0 else ahead, mt),
+            device_id_type=MESH,
+        )
+
+    def advance(piece, step):
+        for way in range(2):
+            if 1 <= step <= hops[piece][way]:
+                ring_copy(piece, way, step - 1).wait_recv()
+            if step < hops[piece][way]:
+                ring_copy(piece, way, step).start()
+
+    rim_copies = []
+    for i, (a, b) in enumerate(((xf_ref, rim_x), (bf_ref, rim_b), (cf_ref, rim_c))):
+        rim_copies.append(
+            pltpu.make_async_remote_copy(
+                src_ref=a.at[pl.ds(rows - RIM, RIM)],
+                dst_ref=b,
+                send_sem=rim_send.at[i],
+                recv_sem=rim_recv.at[i],
+                device_id=((me + 1) % n_sp, mt),
+                device_id_type=MESH,
+            )
+        )
+        rim_copies[-1].start()
+    own_copies = []
+    for piece in range(3):
+        advance(piece, 0)
+        own_copies.append(
+            pltpu.make_async_copy(sources[piece], slot(piece, me), own_sem.at[piece])
+        )
+        own_copies[-1].start()
+
+    raw = dt_ref[...] + doff_ref[...]
+    step_ref[...] = jnp.maximum(raw, 0.0) + jnp.log1p(jnp.exp(-jnp.abs(raw)))
+    ld_ref[...] = elf_ref[...] - fade_ref[...] * step_ref[...]
+
+    for c in rim_copies:
+        c.wait_recv()
+    first = me == 0
+    for rim, feed, taps, act in (
+        (rim_x, xf_ref, xk_ref, x_act),
+        (rim_b, bf_ref, bk_ref, b_act),
+        (rim_c, cf_ref, ck_ref, c_act),
+    ):
+        for lo in range(0, feed.shape[1], 128):
+            here = slice(lo, lo + 128)
+            edge = rim[:, here].astype(f32)
+            ext[0:RIM, :] = jnp.where(first, jnp.zeros_like(edge), edge)
+            ext[RIM:, :] = feed[:, here].astype(f32)
+            tap = taps[:, here].astype(f32)
+            total = jnp.zeros((rows, 128), f32)
+            for k in range(CONV):
+                start = RIM - (CONV - 1) + k
+                total = total + tap[k : k + 1] * ext[start : start + rows, :]
+            act[:, here] = silu(total).astype(bf16)
+
+    li = lax.broadcasted_iota(jnp.int32, (BLOCK, BLOCK), 0)
+    si = lax.broadcasted_iota(jnp.int32, (BLOCK, BLOCK), 1)
+    causal = li >= si
+    lower = jnp.where(causal, 1.0, 0.0).astype(f32)
+    upper = jnp.where(li <= si, 1.0, 0.0).astype(f32)
+    spread = jnp.where(
+        lax.broadcasted_iota(jnp.int32, (heads, inner), 1) // HEAD_DIM
+        == lax.broadcasted_iota(jnp.int32, (heads, inner), 0),
+        1.0,
+        0.0,
+    ).astype(f32)
+    near = lax.broadcasted_iota(jnp.int32, (BLOCK, 2 * HEAD_DIM), 1) < HEAD_DIM
+
+    def widen(a):
+        return jnp.dot(a, spread, precision=HIGHEST, preferred_element_type=f32)
+
+    state_ref[...] = jnp.zeros_like(state_ref)
+    base_ref[...] = jnp.zeros_like(base_ref)
+    skip = widen(byp_ref[...])
+
+    def scan_block(b, carry):
+        at = pl.ds(pl.multiple_of(b * BLOCK, BLOCK), BLOCK)
+        ld = ld_ref[at, :]
+        cum = jnp.dot(lower, ld, precision=HIGHEST, preferred_element_type=f32)
+        cum_t = lax.dot_general(
+            ld, upper, (((0,), (0,)), ((), ())), precision=HIGHEST, preferred_element_type=f32
+        )
+        last = cum[BLOCK - 1 : BLOCK, :]
+        x = x_act[at, :].astype(f32)
+        bb = b_act[at, :]
+        cc = c_act[at, :]
+        xs = x * widen(step_ref[at, :])
+        xs16 = xs.astype(bf16)
+        aff = lax.dot_general(
+            cc, bb, (((1,), (1,)), ((), ())), preferred_element_type=f32
+        )
+        y = (
+            jnp.dot(cc, state_ref[...].astype(bf16), preferred_element_type=f32)
+            * widen(jnp.exp(cum))
+            + skip * x
+        )
+        for pair in range(heads // 2):
+            at_pair = slice(pair * 2 * HEAD_DIM, (pair + 1) * 2 * HEAD_DIM)
+            both = []
+            for h in (2 * pair, 2 * pair + 1):
+                gap = cum[:, h : h + 1] - cum_t[h : h + 1, :]
+                lag = jnp.exp(jnp.where(causal, gap, -1e30))
+                both.append(
+                    jnp.dot(
+                        (aff * lag).astype(bf16), xs16[:, at_pair], preferred_element_type=f32
+                    )
+                )
+            y_ref[at, at_pair] = y[:, at_pair] + jnp.where(near, both[0], both[1])
+        fresh = lax.dot_general(
+            bb,
+            (xs * widen(jnp.exp(last - cum))).astype(bf16),
+            (((0,), (0,)), ((), ())),
+            preferred_element_type=f32,
+        )
+        state_ref[...] = state_ref[...] * widen(jnp.exp(last)) + fresh
+        base = base_ref[0:1, :]
+        efs_ref[at, :] = jnp.exp(base + cum)
+        base_ref[0:1, :] = base + last
+        return carry
+
+    lax.fori_loop(0, blocks, scan_block, 0)
+    st_send[...] = state_ref[...].astype(bf16)
+    dec_send[...] = jnp.broadcast_to(widen(jnp.exp(base_ref[0:1, :])), dec_send.shape)
+
+    def state_copies(d):
+        to = ((me + d) % n_sp, mt)
+        return [
+            pltpu.make_async_remote_copy(
+                src_ref=a,
+                dst_ref=b.at[d],
+                send_sem=st_ssem.at[d, i],
+                recv_sem=st_rsem.at[d, i],
+                device_id=to,
+                device_id_type=MESH,
+            )
+            for i, (a, b) in enumerate(((st_send, st_recv), (dec_send, dec_recv)))
+        ]
+
+    state_ref[...] = jnp.zeros_like(state_ref)
+    for d in range(1, n_sp):
+
+        @pl.when(me + d < n_sp)
+        def _(d=d):
+            for c in state_copies(d):
+                c.start()
+
+    advance(0, 1)
+    advance(1, 1)
+    for d in range(n_sp - 1, 0, -1):
+
+        @pl.when(me >= d)
+        def _(d=d):
+            for c in state_copies(d):
+                c.wait_recv()
+            state_ref[...] = state_ref[...] * dec_recv[d, 0:1, :] + st_recv[d].astype(f32)
+
+    def project_block(b, carry):
+        at = pl.ds(pl.multiple_of(b * BLOCK, BLOCK), BLOCK)
+        y = y_ref[at, :] + jnp.dot(
+            c_act[at, :], state_ref[...].astype(bf16), preferred_element_type=f32
+        ) * widen(efs_ref[at, :])
+        gated = y * silu(rv_ref[at, :].astype(f32))
+        gated = gated * lax.rsqrt(jnp.mean(gated * gated, axis=-1, keepdims=True) + EPSILON)
+        y_norm = (gated * csv_ref[...]).astype(bf16)
+        part[at, :] = jnp.dot(y_norm, mm_ref[...], preferred_element_type=f32).astype(bf16)
+        return carry
+
+    lax.fori_loop(0, blocks, project_block, 0)
+
+    def rows_of(t):
+        return pl.ds(pl.multiple_of(t * own_rows, own_rows), own_rows)
+
+    def tp_copy(d, src, dst, send, recv):
+        return pltpu.make_async_remote_copy(
+            src_ref=src,
+            dst_ref=dst,
+            send_sem=send,
+            recv_sem=recv,
+            device_id=(me, (mt + d) % n_tp),
+            device_id_type=MESH,
+        )
+
+    first_sum = [
+        tp_copy(d, part.at[rows_of((mt + d) % n_tp)], recv1.at[d], t1_send.at[d], t1_recv.at[d])
+        for d in range(1, n_tp)
+    ]
+    for c in first_sum:
+        c.start()
+    advance(0, 2)
+    for c in first_sum:
+        c.wait_recv()
+    mixer = part[rows_of(mt), :].astype(f32)
+    for d in range(1, n_tp):
+        mixer = mixer + recv1[d].astype(f32)
+    mine = pl.ds(pl.multiple_of(RIM + mt * own_rows, RIM), own_rows)
+    normed[mine, :] = layer_norm(
+        ALPHA * res_ref[...].astype(f32) + mixer, g1_ref[...]
+    ).astype(bf16)
+    for c in first_sum:
+        c.wait_send()
+    spread_rows = [
+        tp_copy(d, normed.at[mine], normed.at[mine], t2_send.at[d], t2_recv.at[d])
+        for d in range(1, n_tp)
+    ]
+    for c in spread_rows:
+        c.start()
+    advance(1, 2)
+    advance(0, 3)
+    for c in spread_rows:
+        c.wait()
+    rim_norm = pltpu.make_async_remote_copy(
+        src_ref=normed.at[pl.ds(rows, RIM)],
+        dst_ref=normed.at[pl.ds(0, RIM)],
+        send_sem=nr_send,
+        recv_sem=nr_recv,
+        device_id=((me + 1) % n_sp, mt),
+        device_id_type=MESH,
+    )
+
+    @pl.when(me + 1 < n_sp)
+    def _():
+        rim_norm.start()
+
+    @pl.when(me == 0)
+    def _():
+        normed[0:RIM, :] = jnp.zeros((RIM, width), bf16)
+
+    advance(1, 3)
+    advance(2, 1)
+    for s in range(4, half + 1):
+        advance(0, s)
+        advance(1, s)
+
+    @pl.when(me > 0)
+    def _():
+        rim_norm.wait_recv()
+
+    for c in own_copies:
+        c.wait()
+
+    def ffn_cols(at):
+        feeds = normed[...]
+        convs = []
+        for weights, taps in ((v_all, vk_ref), (w_all, wk_ref)):
+            proj = jnp.dot(feeds, weights[:, at], preferred_element_type=f32)
+            proj = proj.astype(bf16).astype(f32)
+            tap = taps[:, at].astype(f32)
+            total = jnp.zeros((rows, proj.shape[1]), f32)
+            for k in range(FCONV):
+                start = RIM - (FCONV - 1) + k
+                total = total + tap[k : k + 1] * proj[start : start + rows, :]
+            convs.append(total)
+        hidden[:, at] = (silu(convs[0]) * convs[1]).astype(bf16)
+
+    chunk = 256
+    full = ff // chunk
+
+    def ffn_chunk(i, carry):
+        ffn_cols(pl.ds(pl.multiple_of(i * chunk, chunk), chunk))
+        return carry
+
+    lax.fori_loop(0, full // 2, ffn_chunk, 0)
+    advance(2, 2)
+    lax.fori_loop(full // 2, full, ffn_chunk, 0)
+    if ff % chunk:
+        ffn_cols(pl.ds(full * chunk, ff % chunk))
+
+    def down(who):
+        at = pl.ds(pl.multiple_of(who * cols, cols), cols)
+        part[:, at] = jnp.dot(
+            hidden[...], s_all[who], preferred_element_type=f32
+        ).astype(bf16)
+
+    def down_copies(who):
+        at = pl.ds(pl.multiple_of(who * cols, cols), cols)
+        return [
+            tp_copy(
+                d,
+                part.at[rows_of((mt + d) % n_tp), at],
+                recv2.at[d, :, at],
+                t3_send.at[d, who],
+                t3_recv.at[d, who],
+            )
+            for d in range(1, n_tp)
+        ]
+
+    down(me)
+    for c in down_copies(me):
+        c.start()
+    for k in range(1, half + 1):
+        if k >= 3:
+            advance(2, k)
+        count = 2 if k < half else 1
+
+        def both_ways(q, carry, k=k):
+            who = owner((place + n_sp - k + 2 * k * q) % n_sp)
+            down(who)
+            for c in down_copies(who):
+                c.start()
+            return carry
+
+        lax.fori_loop(0, count, both_ways, 0)
+
+    def settle(who, carry):
+        for c in down_copies(who):
+            c.wait()
+        return carry
+
+    lax.fori_loop(0, n_sp, settle, 0)
+    channel = part[rows_of(mt), :].astype(f32)
+    for d in range(1, n_tp):
+        channel = channel + recv2[d].astype(f32)
+    out_ref[...] = layer_norm(
+        ALPHA * normed[mine, :].astype(f32) + channel, g2_ref[...]
+    ).astype(bf16)
+
+    for piece in range(3):
+        for way in range(2):
+            for s in range(hops[piece][way]):
+                ring_copy(piece, way, s).wait_send()
+    for c in rim_copies:
+        c.wait_send()
+
+    @pl.when(me + 1 < n_sp)
+    def _():
+        rim_norm.wait_send()
+
+    for d in range(1, n_sp):
+
+        @pl.when(me + d < n_sp)
+        def _(d=d):
+            for c in state_copies(d):
+                c.wait_send()
+
+
+def fused_shards(n_sp, n_tp, *args):
+    (
+        res, rv, xf, bf, cf, dt, doff, fade, elf, byp, xk, bk, ck, csv, mm, g1, v, w, s, vk, wk, g2
+    ) = args
+    f32, bf16 = jnp.float32, jnp.bfloat16
+    rows, inner = xf.shape
+    heads = dt.shape[1]
+    width = mm.shape[1]
+    ff = v.shape[1]
+    row = lambda a: a.reshape(1, -1)
+    half = n_sp // 2
+    vmem = pl.BlockSpec(memory_space=pltpu.VMEM)
+    hbm = pl.BlockSpec(memory_space=pl.ANY)
+    dma = pltpu.SemaphoreType.DMA
+    return pl.pallas_call(
+        functools.partial(layer_kernel, n_sp, n_tp),
+        out_shape=jax.ShapeDtypeStruct(res.shape, bf16),
+        in_specs=[vmem] * 16 + [hbm] * 3 + [vmem] * 3,
+        out_specs=vmem,
+        scratch_shapes=[
+            pltpu.VMEM((n_sp * v.shape[0], ff), bf16),
+            pltpu.VMEM((n_sp * v.shape[0], ff), bf16),
+            pltpu.VMEM((n_sp,) + s.shape, bf16),
+            pltpu.VMEM((RIM, inner), bf16),
+            pltpu.VMEM((RIM, STATE), bf16),
+            pltpu.VMEM((RIM, STATE), bf16),
+            pltpu.VMEM((rows + RIM, 128), f32),
+            pltpu.VMEM((rows, inner), bf16),
+            pltpu.VMEM((rows, STATE), bf16),
+            pltpu.VMEM((rows, STATE), bf16),
+            pltpu.VMEM((rows, heads), f32),
+            pltpu.VMEM((rows, heads), f32),
+            pltpu.VMEM((rows, inner), f32),
+            pltpu.VMEM((rows, heads), f32),
+            pltpu.VMEM((8, heads), f32),
+            pltpu.VMEM((STATE, inner), f32),
+            pltpu.VMEM((STATE, inner), bf16),
+            pltpu.VMEM((8, inner), f32),
+            pltpu.VMEM((n_sp, STATE, inner), bf16),
+            pltpu.VMEM((n_sp, 8, inner), f32),
+            pltpu.VMEM((rows, width), bf16),
+            pltpu.VMEM((n_tp, rows // n_tp, width), bf16),
+            pltpu.VMEM((n_tp, rows // n_tp, width), bf16),
+            pltpu.VMEM((rows + RIM, width), bf16),
+            pltpu.VMEM((rows, ff), bf16),
+            dma((3,)),
+            dma((2, half, 3)),
+            dma((2, half, 3)),
+            dma((3,)),
+            dma((3,)),
+            dma((n_sp, 2)),
+            dma((n_sp, 2)),
+            dma((n_tp,)),
+            dma((n_tp,)),
+            dma((n_tp,)),
+            dma((n_tp,)),
+            dma((n_tp, n_sp)),
+            dma((n_tp, n_sp)),
+            dma,
+            dma,
+        ],
+        compiler_params=pltpu.CompilerParams(
+            collective_id=0, has_side_effects=True, vmem_limit_bytes=60 * 1024 * 1024
+        ),
+    )(
+        res, rv, xf, bf, cf, dt, row(doff), row(fade), elf, row(byp), xk, bk, ck, row(csv), mm,
+        row(g1), v, w, s, vk, wk, row(g2),
+    )
+
+
+def shards_for(n_sp, n_tp):
+    def shards(*args):
+        rows = args[2].shape[0]
+        fits = (
+            args[3].shape[1] == STATE
+            and args[18].shape[1] % 128 == 0
+            and args[16].shape[0] % 16 == 0
+            and args[16].shape[1] % 128 == 0
+            and n_sp % 2 == 0
+            and rows % (BLOCK * n_tp) == 0
+        )
+        if fits:
+            return fused_shards(n_sp, n_tp, *args)
+        return plain_shards(*args)
+
+    return shards
+
+
 def solution(mesh):
     in_specs = (
         P(("sp", "tp"), None),
@@ -245,4 +795,5 @@
         P(),
     )
     out_specs = P(("sp", "tp"), None)
+    shards = shards_for(mesh.shape["sp"], mesh.shape["tp"])
     return jax.shard_map(shards, mesh=mesh, in_specs=in_specs, out_specs=out_specs, check_vma=False)

time: 509 us -> 216 us (0.42)
  waiting for transfers between devices: 353 us -> 0 us
  Pallas kernels: 0 us -> 211 us
  other arithmetic: 50.6 us -> 0 us
  matrix products: 43.8 us -> 0 us
  local copies, waits for them, and re-layouts: 19.3 us -> 4.99 us
  between operations: 13.9 us -> 0.01 us
  blocking collectives: 13.3 us -> 0 us
  starting transfers between devices: 11.7 us -> 0 us
    all_gather x5 -> x0, waiting for transfers between devices: 285 us -> none  [the longest x1 92.2 us: shards(): lax.all_gather(valve_matrix, 'sp', axis=0, tiled=True)]
    pallas_call x0 -> x1, Pallas kernels: none -> 211 us  [fused_shards(): pl.pallas_call(functools.partial(layer_kernel, n_sp, n_tp), out_shape=jax...]
    reduce_scatter x2 -> x0, waiting for transfers between devices: 65.9 us -> none  [the longest x1 34.7 us: shards(): lax.psum_scatter(jnp.dot(y_norm, mixer_result_matrix, preferred_element_t...]
    dot_general x9 -> x0, matrix products: 43.8 us -> none  [the longest x1 14.5 us: shards(): jnp.dot(hidden, lax.all_gather(shrink_matrix, 'sp', axis=1, tiled=True),...]
    convert_element_type x17 -> x0, other arithmetic: 18.4 us -> none  [the longest x5 7.06 us: causal_conv(): padded = jnp.concatenate([before, signal], axis=0).astype(jnp.float32)]
    all_gather x1 -> x0, blocking collectives: 13.3 us -> none  [entering(): lax.all_gather(a.astype(kind), axis)]
    ppermute x5 -> x0, starting transfers between devices: 11.3 us -> none  [shifted(): return lax.ppermute(shard, axis, pairs)]
    add x10 -> x0, other arithmetic: 10.2 us -> none  [the longest x6 6.06 us: combine_states(): earlier_pair[0] * later_pair[1][..., None, None] + later_pair[0]]
  transfers between devices with their start and end apart: 12 -> 0, of which waited for: 8 -> 0; matrix products, arithmetic and copies ran while one was open for 13% -> 0% of each run, Pallas kernels for 0% -> 0%
where the time goes in v1:
time: 216 us
  Pallas kernels  211 us (98%)
  local copies, waits for them, and re-layouts  4.99 us (2%)
    pallas_call x1, Pallas kernels, fused_shards(): pl.pallas_call(functools.partial(layer_kernel, n_sp, n_tp), out_shape=jax...  211 us
    unnamed x3, local copies, waits for them, and re-layouts  4.99 us

profile of v1, /device:TPU:25, one launch (start us, length us, event | category | flops | bytes accessed | tf_op | source)
XLA Modules:
  0.0 215.6 jit_solution(17617308902706226636)
XLA Ops:
  0.0 1.6 copy.23.dt_ref
  1.6 1.6 copy.24.elf_ref
  3.1 210.6 %shard_map.208 = bf16[128,2048]{1,0:T(8,128)(2,1)} custom-call(bf16[128,2048]{1,0:T(8,128)(2,1)} %res_ref.1, bf16[512,512]{1,0:T(8,128)(2,1)} %rv_ref.1, bf16[512,512]{1,0:T(8,128)(2,1)} %xf_ref.1, bf16[512,128]{1,0:T(8,128)(2,1)} %bf_ref.1, bf16[512,128]{1,0:T(8,128)(2,1)} %cf_ref.1, f32[512,8]{1,0:T(8,128)} %copy.23.dt_ref, f32[1,8]{1,0:T(1,128)} %bitcast.9, ...), custom_call_target="tpu_custom_call" | custom-call | tf_op jit(solution)/shard_map/pallas_call | solution.py:698
  213.8 1.9 copy.26

commit v2 on v1

--- a/solution.py
+++ b/solution.py
@@ -274,6 +274,8 @@
     state_ref,
     st_send,
     dec_send,
+    pair_send,
+    pair_dec,
     st_recv,
     dec_recv,
     part,
@@ -336,13 +338,19 @@
     hops = {}
     for piece in range(3):
         long_way = half if piece != 1 else n_sp - 1 - half
-        hops[piece] = (long_way, n_sp - 1 - long_way)
+        hops[piece] = (long_way, n_sp - 1 - long_way) if piece < 2 else (half, half)
 
     def ring_copy(piece, way, step):
         who = owner((place + n_sp - step) % n_sp if way == 0 else (place + step) % n_sp)
+        src = sources[piece] if step == 0 else slot(piece, who)
+        dst = slot(piece, who)
+        if piece == 2 and step == half - 1:
+            part_rows = src.shape[0] // 2
+            here = pl.ds(way * part_rows, part_rows)
+            src, dst = src.at[here], dst.at[here]
         return pltpu.make_async_remote_copy(
-            src_ref=sources[piece] if step == 0 else slot(piece, who),
-            dst_ref=slot(piece, who),
+            src_ref=src,
+            dst_ref=dst,
             send_sem=ring_send.at[way, step, piece],
             recv_sem=ring_recv.at[way, step, piece],
             device_id=(after if way == 0 else ahead, mt),
@@ -371,7 +379,8 @@
         rim_copies[-1].start()
     own_copies = []
     for piece in range(3):
-        advance(piece, 0)
+        if piece < 2:
+            advance(piece, 0)
         own_copies.append(
             pltpu.make_async_copy(sources[piece], slot(piece, me), own_sem.at[piece])
         )
@@ -468,39 +477,63 @@
 
     lax.fori_loop(0, blocks, scan_block, 0)
     st_send[...] = state_ref[...].astype(bf16)
-    dec_send[...] = jnp.broadcast_to(widen(jnp.exp(base_ref[0:1, :])), dec_send.shape)
+    dec_send[...] = jnp.broadcast_to(base_ref[0:1, :], dec_send.shape)
+    partner = me + 1 - 2 * odd
 
     def state_copies(d):
-        to = ((me + d) % n_sp, mt)
+        pair = d > 0
         return [
             pltpu.make_async_remote_copy(
                 src_ref=a,
                 dst_ref=b.at[d],
                 send_sem=st_ssem.at[d, i],
                 recv_sem=st_rsem.at[d, i],
-                device_id=to,
+                device_id=((me + 2 * d) % n_sp if pair else partner, mt),
                 device_id_type=MESH,
             )
-            for i, (a, b) in enumerate(((st_send, st_recv), (dec_send, dec_recv)))
+            for i, (a, b) in enumerate(
+                ((pair_send if pair else st_send, st_recv), (pair_dec if pair else dec_send, dec_recv))
+            )
         ]
 
+    for c in state_copies(0):
+        c.start()
+    advance(0, 1)
+    for c in state_copies(0):
+        c.wait_recv()
+    own_dec = widen(jnp.exp(dec_send[0:1, :]))
+    beside_dec = widen(jnp.exp(dec_recv[0, 0:1, :]))
+    beside = st_recv[0].astype(f32)
+    later = odd == 1
+    pair_send[...] = jnp.where(
+        later, state_ref[...] + beside * own_dec, state_ref[...] * beside_dec + beside
+    ).astype(bf16)
+    pair_dec[...] = dec_send[...] + dec_recv[0]
     state_ref[...] = jnp.zeros_like(state_ref)
-    for d in range(1, n_sp):
-
-        @pl.when(me + d < n_sp)
+    for d in range(1, half):
+
+        @pl.when(me + 2 * d < n_sp)
         def _(d=d):
             for c in state_copies(d):
                 c.start()
 
-    advance(0, 1)
     advance(1, 1)
-    for d in range(n_sp - 1, 0, -1):
-
-        @pl.when(me >= d)
+    advance(2, 0)
+    for d in range(half - 1, 0, -1):
+
+        @pl.when(me >= 2 * d)
         def _(d=d):
             for c in state_copies(d):
                 c.wait_recv()
-            state_ref[...] = state_ref[...] * dec_recv[d, 0:1, :] + st_recv[d].astype(f32)
+            state_ref[...] = state_ref[...] * widen(
+                jnp.exp(dec_recv[d, 0:1, :])
+            ) + st_recv[d].astype(f32)
+
+    @pl.when(odd == 1)
+    def _():
+        state_ref[...] = state_ref[...] * widen(jnp.exp(dec_recv[0, 0:1, :])) + st_recv[
+            0
+        ].astype(f32)
 
     def project_block(b, carry):
         at = pl.ds(pl.multiple_of(b * BLOCK, BLOCK), BLOCK)
@@ -673,9 +706,11 @@
     def _():
         rim_norm.wait_send()
 
-    for d in range(1, n_sp):
-
-        @pl.when(me + d < n_sp)
+    for c in state_copies(0):
+        c.wait_send()
+    for d in range(1, half):
+
+        @pl.when(me + 2 * d < n_sp)
         def _(d=d):
             for c in state_copies(d):
                 c.wait_send()
@@ -718,9 +753,11 @@
             pltpu.VMEM((8, heads), f32),
             pltpu.VMEM((STATE, inner), f32),
             pltpu.VMEM((STATE, inner), bf16),
-            pltpu.VMEM((8, inner), f32),
-            pltpu.VMEM((n_sp, STATE, inner), bf16),
-            pltpu.VMEM((n_sp, 8, inner), f32),
+            pltpu.VMEM((8, heads), f32),
+            pltpu.VMEM((STATE, inner), bf16),
+            pltpu.VMEM((8, heads), f32),
+            pltpu.VMEM((half, STATE, inner), bf16),
+            pltpu.VMEM((half, 8, heads), f32),
             pltpu.VMEM((rows, width), bf16),
             pltpu.VMEM((n_tp, rows // n_tp, width), bf16),
             pltpu.VMEM((n_tp, rows // n_tp, width), bf16),
@@ -731,8 +768,8 @@
             dma((2, half, 3)),
             dma((3,)),
             dma((3,)),
-            dma((n_sp, 2)),
-            dma((n_sp, 2)),
+            dma((half, 2)),
+            dma((half, 2)),
             dma((n_tp,)),
             dma((n_tp,)),
             dma((n_tp,)),
@@ -760,6 +797,8 @@
             and args[16].shape[0] % 16 == 0
             and args[16].shape[1] % 128 == 0
             and n_sp % 2 == 0
+            and n_sp >= 4
+            and args[18].shape[0] % 32 == 0
             and rows % (BLOCK * n_tp) == 0
         )
         if fits:

time: 216 us -> 197 us (0.912); the launches traced: 216 us -> 194 us
  Pallas kernels: 211 us -> 189 us
    pallas_call x1, Pallas kernels: 211 us -> 189 us  [fused_shards(): pl.pallas_call(functools.partial(layer_kernel, n_sp, n_tp), out_shape=jax...]
where the time goes in v2:
time: 197 us; the launch traced here: 194 us
  Pallas kernels  189 us (96%)
  local copies, waits for them, and re-layouts  4.99 us (3%)
    pallas_call x1, Pallas kernels, fused_shards(): pl.pallas_call(functools.partial(layer_kernel, n_sp, n_tp), out_shape=jax...  189 us
    unnamed x3, local copies, waits for them, and re-layouts  4.99 us

profile of v2, /device:TPU:25, one launch (start us, length us, event | category | flops | bytes accessed | tf_op | source)
XLA Modules:
  0.0 194.4 jit_solution(8849307077106910371)
XLA Ops:
  0.0 1.6 copy.23.dt_ref
  1.6 1.6 copy.24.elf_ref
  3.1 189.4 %shard_map.208 = bf16[128,2048]{1,0:T(8,128)(2,1)} custom-call(bf16[128,2048]{1,0:T(8,128)(2,1)} %res_ref.1, bf16[512,512]{1,0:T(8,128)(2,1)} %rv_ref.1, bf16[512,512]{1,0:T(8,128)(2,1)} %xf_ref.1, bf16[512,128]{1,0:T(8,128)(2,1)} %bf_ref.1, bf16[512,128]{1,0:T(8,128)(2,1)} %cf_ref.1, f32[512,8]{1,0:T(8,128)} %copy.23.dt_ref, f32[1,8]{1,0:T(1,128)} %bitcast.9, ...), custom_call_target="tpu_custom_call" | custom-call | tf_op jit(solution)/shard_map/pallas_call | solution.py:733
  192.5 1.9 copy.26

commit v3 on v2

--- a/solution.py
+++ b/solution.py
@@ -233,8 +233,8 @@
 def layer_kernel(
     n_sp,
     n_tp,
-    res_ref,
-    rv_ref,
+    res_hbm,
+    rv_hbm,
     xf_ref,
     bf_ref,
     cf_ref,
@@ -247,7 +247,7 @@
     bk_ref,
     ck_ref,
     csv_ref,
-    mm_ref,
+    mm_hbm,
     g1_ref,
     v_hbm,
     w_hbm,
@@ -283,6 +283,10 @@
     recv2,
     normed,
     hidden,
+    res_ref,
+    rv_ref,
+    mm_ref,
+    late_sem,
     own_sem,
     ring_send,
     ring_recv,
@@ -301,9 +305,9 @@
 ):
     f32, bf16 = jnp.float32, jnp.bfloat16
     rows, inner = xf_ref.shape
-    heads = dt_ref.shape[1]
+    heads = dt_ref.shape[0]
     own_rows = rows // n_tp
-    width = mm_ref.shape[1]
+    width = mm_hbm.shape[1]
     ff = v_hbm.shape[1]
     depth = v_hbm.shape[0]
     cols = s_hbm.shape[1]
@@ -386,9 +390,23 @@
         )
         own_copies[-1].start()
 
-    raw = dt_ref[...] + doff_ref[...]
+    late = [
+        pltpu.make_async_copy(a, b, late_sem.at[i])
+        for i, (a, b) in enumerate(((rv_hbm, rv_ref), (mm_hbm, mm_ref), (res_hbm, res_ref)))
+    ]
+    for c in late:
+        c.start()
+
+    eye = lax.broadcasted_iota(jnp.int32, (heads, heads), 0) == lax.broadcasted_iota(
+        jnp.int32, (heads, heads), 1
+    )
+
+    def column(a):
+        return jnp.sum(jnp.where(eye, a[...], 0.0), axis=1, keepdims=True)
+
+    raw = dt_ref[...] + column(doff_ref)
     step_ref[...] = jnp.maximum(raw, 0.0) + jnp.log1p(jnp.exp(-jnp.abs(raw)))
-    ld_ref[...] = elf_ref[...] - fade_ref[...] * step_ref[...]
+    ld_ref[...] = elf_ref[...] - column(fade_ref) * step_ref[...]
 
     for c in rim_copies:
         c.wait_recv()
@@ -432,16 +450,22 @@
 
     def scan_block(b, carry):
         at = pl.ds(pl.multiple_of(b * BLOCK, BLOCK), BLOCK)
-        ld = ld_ref[at, :]
-        cum = jnp.dot(lower, ld, precision=HIGHEST, preferred_element_type=f32)
-        cum_t = lax.dot_general(
-            ld, upper, (((0,), (0,)), ((), ())), precision=HIGHEST, preferred_element_type=f32
-        )
+        ld = ld_ref[:, at]
+        cum = lax.dot_general(
+            lower, ld, (((1,), (1,)), ((), ())), precision=HIGHEST, preferred_element_type=f32
+        )
+        cum_t = jnp.dot(ld, upper, precision=HIGHEST, preferred_element_type=f32)
         last = cum[BLOCK - 1 : BLOCK, :]
         x = x_act[at, :].astype(f32)
         bb = b_act[at, :]
         cc = c_act[at, :]
-        xs = x * widen(step_ref[at, :])
+        xs = x * lax.dot_general(
+            step_ref[:, at],
+            spread,
+            (((0,), (0,)), ((), ())),
+            precision=HIGHEST,
+            preferred_element_type=f32,
+        )
         xs16 = xs.astype(bf16)
         aff = lax.dot_general(
             cc, bb, (((1,), (1,)), ((), ())), preferred_element_type=f32
@@ -534,6 +558,9 @@
         state_ref[...] = state_ref[...] * widen(jnp.exp(dec_recv[0, 0:1, :])) + st_recv[
             0
         ].astype(f32)
+
+    for c in late:
+        c.wait()
 
     def project_block(b, carry):
         at = pl.ds(pl.multiple_of(b * BLOCK, BLOCK), BLOCK)
@@ -733,7 +760,7 @@
     return pl.pallas_call(
         functools.partial(layer_kernel, n_sp, n_tp),
         out_shape=jax.ShapeDtypeStruct(res.shape, bf16),
-        in_specs=[vmem] * 16 + [hbm] * 3 + [vmem] * 3,
+        in_specs=[hbm] * 2 + [vmem] * 12 + [hbm, vmem] + [hbm] * 3 + [vmem] * 3,
         out_specs=vmem,
         scratch_shapes=[
             pltpu.VMEM((n_sp * v.shape[0], ff), bf16),
@@ -746,8 +773,8 @@
             pltpu.VMEM((rows, inner), bf16),
             pltpu.VMEM((rows, STATE), bf16),
             pltpu.VMEM((rows, STATE), bf16),
-            pltpu.VMEM((rows, heads), f32),
-            pltpu.VMEM((rows, heads), f32),
+            pltpu.VMEM((heads, rows), f32),
+            pltpu.VMEM((heads, rows), f32),
             pltpu.VMEM((rows, inner), f32),
             pltpu.VMEM((rows, heads), f32),
             pltpu.VMEM((8, heads), f32),
@@ -763,6 +790,10 @@
             pltpu.VMEM((n_tp, rows // n_tp, width), bf16),
             pltpu.VMEM((rows + RIM, width), bf16),
             pltpu.VMEM((rows, ff), bf16),
+            pltpu.VMEM(res.shape, bf16),
+            pltpu.VMEM(rv.shape, bf16),
+            pltpu.VMEM(mm.shape, bf16),
+            dma((3,)),
             dma((3,)),
             dma((2, half, 3)),
             dma((2, half, 3)),
@@ -783,7 +814,7 @@
             collective_id=0, has_side_effects=True, vmem_limit_bytes=60 * 1024 * 1024
         ),
     )(
-        res, rv, xf, bf, cf, dt, row(doff), row(fade), elf, row(byp), xk, bk, ck, row(csv), mm,
+        res, rv, xf, bf, cf, dt.T, row(doff), row(fade), elf.T, row(byp), xk, bk, ck, row(csv), mm,
         row(g1), v, w, s, vk, wk, row(g2),
     )
 

time: 197 us -> 193 us (0.980)
  local copies, waits for them, and re-layouts: 4.99 us -> 1.88 us
    unnamed x3 -> x1, local copies, waits for them, and re-layouts: 4.99 us -> 1.88 us
where the time goes in v3:
time: 193 us; the launch traced here: 190 us
  Pallas kernels  188 us (97%)
    pallas_call x1, Pallas kernels, fused_shards(): pl.pallas_call(functools.partial(layer_kernel, n_sp, n_tp), out_shape=jax...  188 us

profile of v3, /device:TPU:25, one launch (start us, length us, event | category | flops | bytes accessed | tf_op | source)
XLA Modules:
  0.0 190.2 jit_solution(3608524297670995484)
XLA Ops:
  0.0 188.3 %shard_map.208 = bf16[128,2048]{1,0:T(8,128)(2,1)} custom-call(bf16[128,2048]{1,0:T(8,128)(2,1)} %res_hbm.1, bf16[512,512]{1,0:T(8,128)(2,1)} %rv_hbm.1, bf16[512,512]{1,0:T(8,128)(2,1)} %xf_ref.1, bf16[512,128]{1,0:T(8,128)(2,1)} %bf_ref.1, bf16[512,128]{1,0:T(8,128)(2,1)} %cf_ref.1, f32[8,512]{1,0:T(8,128)} %bitcast.8, f32[1,8]{1,0:T(1,128)} %bitcast.13, ...), custom_call_target="tpu_custom_call" | custom-call | tf_op jit(solution)/shard_map/pallas_call | solution.py:760
  188.3 1.9 copy.24
